TPU v7x, 32 devices: a whole 2x2x4 slice. The times are simulated.
32 devices in a mesh: ep: 4 (over z), tp: 8 (over y, x, core).
Axes of the slice: x: 2, y: 2, z: 4, core: 2. Of those that a mesh axis runs over, the one named last changes fastest.
Arguments:
- tokens: bfloat16 [672, 2048], P('ep', 'tp'), may hold values from -540 to 540
- norm_gain: float32 [2048], P('tp'), may hold values from 0.1 to 1.9
- chosen: int32 [4, 504], P('ep'), may hold values from 0 to 671, as said below
- affinity: float32 [4, 504], P('ep'), may hold values from 0.1 to 1
- w_gate: bfloat16 [4, 2048, 8192], P('ep', None, 'tp'), may hold values from -0.125 to 0.125
- w_up: bfloat16 [4, 2048, 8192], P('ep', None, 'tp'), may hold values from -0.125 to 0.125
- w_down: bfloat16 [4, 8192, 2048], P('ep', 'tp'), may hold values from -0.0625 to 0.0625
Outputs:
- expert_mix: bfloat16 [672, 2048], P('ep', 'tp')
Inputs may be any that keep to these rules, and one draw needn't show every extreme that they name: `chosen`: each expert's 504 token numbers are distinct. Among one expert's choices at most 168 are tokens of one index of ep, and that bound is reached in every draw.
All inputs are finite; a program needn't handle non-finite values.
Results may differ from a plain program's by a relative error of at most 0.025.
Values may be sent and summed in bfloat16 or wider, within the bound.
A program may use at most 64 MiB of HBM per device.

v0:
```python
import jax
import jax.numpy as jnp
from jax import lax
from jax.sharding import PartitionSpec as P

D = 2048


EPS = 1e-06


def local(tokens, norm_gain, chosen, affinity, w_gate, w_up, w_down):
    tok_dev, width_part = tokens.shape
    ep_count = lax.axis_size("ep")
    floats = tokens.astype(jnp.float32)
    square_sum = lax.psum(jnp.sum(floats * floats, axis=1), "tp")
    normed = (floats * lax.rsqrt(square_sum / D + EPS)[:, None] * norm_gain[None, :]).astype(
        jnp.bfloat16
    )
    own_choice = chosen[0]
    chosen_count = own_choice.shape[0]
    bound_rows = min(tok_dev, 2 * chosen_count // ep_count)
    slot_ids = jnp.arange(bound_rows, dtype=jnp.int32)
    positions = jnp.arange(chosen_count, dtype=jnp.int32)
    every_token = lax.all_gather(normed, "ep", axis=0, tiled=True)
    picked = every_token[own_choice]
    piece = lax.all_gather(picked, "tp", axis=1, tiled=True)
    gate_rows = w_gate[0]
    up_rows = w_up[0]
    gate = jnp.dot(piece, gate_rows, preferred_element_type=jnp.float32)
    upward = jnp.dot(piece, up_rows, preferred_element_type=jnp.float32)
    hidden = (jax.nn.silu(gate) * upward).astype(jnp.bfloat16)
    columns = w_down[0]
    summed = lax.psum_scatter(
        lax.dot_general(
            columns, hidden, (((0,), (1,)), ((), ())), preferred_element_type=jnp.float32
        ).astype(jnp.bfloat16),
        "tp",
        scatter_dimension=0,
        tiled=True,
    ).astype(jnp.float32)
    weighted = (summed * affinity[0][None, :]).astype(jnp.bfloat16).T
    owner = own_choice // tok_dev
    owner_local = own_choice - owner * tok_dev
    owner_hot = owner[:, None] == jnp.arange(ep_count, dtype=jnp.int32)[None, :]
    running = jnp.cumsum(owner_hot.astype(jnp.int32), axis=0)
    place = jnp.sum(jnp.where(owner_hot, running, 0), axis=1) - 1
    back_match = owner_hot.T[:, None, :] & (place[None, None, :] == slot_ids[None, :, None])
    back_filled = jnp.any(back_match, axis=2)
    back_pick = jnp.sum(jnp.where(back_match, positions[None, None, :], 0), axis=2)
    back_rows = jnp.where(back_filled[..., None], weighted[back_pick], jnp.zeros((), jnp.bfloat16))
    back_token = jnp.where(back_filled, owner_local[back_pick], tok_dev)
    got_back, got_token = (
        lax.all_to_all(back_rows, "ep", split_axis=0, concat_axis=0, tiled=True),
        lax.all_to_all(back_token, "ep", split_axis=0, concat_axis=0, tiled=True),
    )
    total = jnp.zeros((tok_dev, width_part), jnp.float32)
    total = total.at[got_token.reshape(-1)].add(
        got_back.reshape(-1, width_part).astype(jnp.float32), mode="drop"
    )
    return total.astype(jnp.bfloat16)


def solution(mesh):
    in_specs = (
        P("ep", "tp"),
        P("tp"),
        P("ep", None),
        P("ep", None),
        P("ep", None, "tp"),
        P("ep", None, "tp"),
        P("ep", "tp", None),
    )
    out_specs = P("ep", "tp")
    return jax.shard_map(local, mesh=mesh, in_specs=in_specs, out_specs=out_specs, check_vma=False)
```

profile of v0, /device:TPU:0, one launch (start us, length us, event | category | flops | bytes accessed | tf_op | source)
XLA Modules:
  0.0 159.4 jit_solution(16379696809128287632)
XLA Ops:
  6.5 1.0 fusion.20
  7.5 15.2 %psum.7 = f32[168]{0:T(256)S(1)} all-reduce(f32[168]{0:T(256)S(1)} %fusion.20), channel_id=1, replica_groups=mesh['ep'=4,'tp'=8] {'tp'}, use_global_device_ids=true, to_apply=%region_6.7 | all-reduce | flops 168 | bytes 1344 | tf_op jit(solution)/shard_map/psum | solution.py:16
  22.7 0.7 compare_select_fusion.1
  23.4 1.0 fusion.22
  24.4 15.0 %all_gather.6 = bf16[672,256]{1,0:T(8,128)(2,1)S(1)} all-gather(bf16[168,256]{1,0:T(8,128)(2,1)S(1)} %fusion.22), channel_id=1, replica_groups=mesh['ep'=4,'tp'=8] {'ep'}, dimensions={0}, use_global_device_ids=true | all-gather | bytes 430080 | tf_op jit(solution)/shard_map/all_gather | solution.py:25
  39.4 2.6 %gather_fusion.1 = bf16[504,256]{1,0:T(8,128)(2,1)} fusion(bf16[672,256]{1,0:T(8,128)(2,1)S(1)} %all_gather.6, s32[1024]{0:T(1024)S(1)} %pad_clamp_fusion), kind=kCustom, calls=%fused_computation.1 | custom fusion | bytes 518112 | tf_op jit(solution)/shard_map/gather | solution.py:26
  42.0 26.9 %all-gather.3.cloned.1.call-done = bf16[504,2048]{1,0:T(8,128)(2,1)} async-done(((bf16[504,256]{1,0:T(8,128)(2,1)}), bf16[504,2048]{1,0:T(8,128)(2,1)}) %all-gather.3.cloned.1.call-update) | async-done | bytes 2064400 | tf_op jit(solution)/shard_map/all_gather | solution.py:27
  68.9 6.5 %fusion.4 = f32[504,1024]{1,0:T(8,128)} fusion(bf16[504,2048]{1,0:T(8,128)(2,1)} %all-gather.3.cloned.1.call-done, bf16[1,2048,1024]{2,1,0:T(8,128)(2,1)} %param.11), kind=kOutput, calls=%fused_computation.8 | convolution fusion | flops 2113929216 | bytes 8323072 | tf_op jit(solution)/shard_map/dot_general | solution.py:30
  75.4 9.8 %fusion.9 = bf16[2048,504]{0,1:T(8,128)(2,1)} fusion(bf16[1,1024,2048]{2,1,0:T(8,128)(2,1)} %param.13, f32[504,1024]{1,0:T(8,128)} %fusion.4, bf16[504,2048]{1,0:T(8,128)(2,1)S(1)} %copy-done.2, bf16[1,2048,1024]{2,1,0:T(8,128)(2,1)} %param.12), kind=kOutput, calls=%fused_computation.11 | convolution fusion | flops 4231987200 | bytes 14581760 | tf_op jit(solution)/shard_map/dot_general | solution.py:35
  85.3 0.7 copy-done
  86.0 1.2 reduce-window.6
  87.8 0.3 fusion.14
  88.3 4.7 %gather_fusion = s32[672]{0:T(1024)S(1)} fusion(s32[504]{0:T(512)S(1)} %get-tuple-element.5, s32[1024]{0:T(1024)S(1)} %pad_clamp_fusion.1), kind=kCustom, calls=%fused_computation | custom fusion | bytes 8064 | tf_op jit(solution)/shard_map/gather | solution.py:52
  93.0 0.2 and_reduce_fusion
  93.3 0.6 copy.8
  93.9 4.6 %all-to-all-start = ((s32[4,1,168]{2,1,0:T(1,128)}), s32[4,1,168]{2,1,0:T(1,128)S(1)}, u32[]{:S(2)}, u32[]{:S(2)}) async-start(s32[4,1,168]{2,1,0:T(1,128)} %copy.8), calls=%async_computation | async-start | bytes 8192 | tf_op jit(solution)/shard_map/all_to_all | solution.py:55
  98.5 27.1 %reduce-scatter.2.cloned.1.call-done = bf16[256,504]{0,1:T(8,128)(2,1)} async-done(((bf16[2048,504]{0,1:T(8,128)(2,1)}), bf16[256,504]{0,1:T(8,128)(2,1)}) %reduce-scatter.2.cloned.1.call-update) | async-done | bytes 258064 | tf_op jit(solution)/shard_map/reduce_scatter | solution.py:34
  125.6 1.1 fusion.19
  126.7 2.8 %gather_fusion.2 = bf16[672,256]{1,0:T(8,128)(2,1)S(1)} fusion(bf16[504,256]{1,0:T(8,128)(2,1)S(1)} %fusion.19, s32[1024]{0:T(1024)S(1)} %pad_clamp_fusion.1), kind=kCustom, calls=%fused_computation.2 | custom fusion | bytes 690816 | tf_op jit(solution)/shard_map/gather | solution.py:51
  129.5 0.9 broadcast_select_fusion
  130.4 4.6 %all-to-all-start.1 = ((bf16[4,168,256]{2,1,0:T(8,128)(2,1)}), bf16[4,168,256]{2,1,0:T(8,128)(2,1)S(1)}, u32[]{:S(2)}, u32[]{:S(2)}) async-start(bf16[4,168,256]{2,1,0:T(8,128)(2,1)} %broadcast_select_fusion), calls=%async_computation.2 | async-start | bytes 688128 | tf_op jit(solution)/shard_map/all_to_all | solution.py:54
  135.1 10.4 %all-to-all-done.1 = bf16[4,168,256]{2,1,0:T(8,128)(2,1)S(1)} async-done(((bf16[4,168,256]{2,1,0:T(8,128)(2,1)}), bf16[4,168,256]{2,1,0:T(8,128)(2,1)S(1)}, u32[]{:S(2)}, u32[]{:S(2)}) %all-to-all-start.1) | async-done | bytes 344096 | tf_op jit(solution)/shard_map/all_to_all | solution.py:54
  145.5 6.4 %scatter_custom_fusion = f32[168,256]{1,0:T(8,128)S(1)} fusion(s32[672]{0:T(1024)S(1)} %fusion.25, bf16[672,256]{1,0:T(8,128)(2,1)S(1)} %bitcast.47, f32[]{:T(128)} %constant.12.clone.1), kind=kCustom, calls=%fused_computation.16 | custom fusion | flops 344064 | bytes 516100 | tf_op jit(solution)/shard_map/scatter-add | solution.py:58
  151.9 0.6 convert_element_type.41
  (31 shorter events, 1.0 us)
Async XLA Ops:
  6.5 62.3 %all-gather.3.cloned.1.call-start = ((), (), s32[]{:S(2)}) async-start(), calls=%async_computation.4 | async-start | bytes 2322432 | tf_op jit(solution)/shard_map/all_gather | solution.py:27
  42.0 83.6 %reduce-scatter.2.cloned.1.call-start = ((), (), s32[]{:S(2)}) async-start(), calls=%async_computation.3 | async-start | bytes 2322432 | tf_op jit(solution)/shard_map/reduce_scatter | solution.py:34
  68.9 6.5 %copy-start.2 = (bf16[504,2048]{1,0:T(8,128)(2,1)S(1)}, bf16[504,2048]{1,0:T(8,128)(2,1)}, u32[]{:S(2)}) copy-start(bf16[504,2048]{1,0:T(8,128)(2,1)} %all-gather.3.cloned.1.call-done) | copy-start | bytes 6193156
  85.3 0.7 copy-start
  88.3 37.3 %copy-start.1 = (f32[1,504]{1,0:T(1,128)S(1)}, f32[1,504]{1,0:T(1,128)}, u32[]{:S(2)}) copy-start(f32[1,504]{1,0:T(1,128)} %param.10) | copy-start | bytes 6052
  93.9 36.5 %all-to-all-start = ((s32[4,1,168]{2,1,0:T(1,128)}), s32[4,1,168]{2,1,0:T(1,128)S(1)}, u32[]{:S(2)}, u32[]{:S(2)}) async-start(s32[4,1,168]{2,1,0:T(1,128)} %copy.8), calls=%async_computation | async-start | bytes 8192 | tf_op jit(solution)/shard_map/all_to_all | solution.py:55
  130.4 15.1 %all-to-all-start.1 = ((bf16[4,168,256]{2,1,0:T(8,128)(2,1)}), bf16[4,168,256]{2,1,0:T(8,128)(2,1)S(1)}, u32[]{:S(2)}, u32[]{:S(2)}) async-start(bf16[4,168,256]{2,1,0:T(8,128)(2,1)} %broadcast_select_fusion), calls=%async_computation.2 | async-start | bytes 688128 | tf_op jit(solution)/shard_map/all_to_all | solution.py:54
Sparse Core Ops, SparseCore 0:
  42.1 26.7 all-gather.2
  85.4 40.1 reduce-scatter.1
where the time goes:
time: 160 us; the launch traced here: 159 us
  waiting for transfers between devices  64.4 us (40%)
  blocking collectives  30.1 us (19%)
  matrix products  16.4 us (10%)
  other arithmetic  13.9 us (9%)
  between operations  13.5 us (8%)
  local copies, waits for them, and re-layouts  11.8 us (7%)
  starting transfers between devices  9.24 us (6%)
    reduce_scatter x1, waiting for transfers between devices, local(): lax.psum_scatter(lax.dot_general(columns, hidden, (((0,), (1,)), ((), ())...  27.1 us
    all_gather x1, waiting for transfers between devices, local(): piece = lax.all_gather(picked, 'tp', axis=1, tiled=True)  26.9 us
    psum x1, blocking collectives, local(): square_sum = lax.psum(jnp.sum(floats * floats, axis=1), 'tp')  15.2 us
    all_gather x1, blocking collectives, local(): every_token = lax.all_gather(normed, 'ep', axis=0, tiled=True)  15 us
    all_to_all x1, waiting for transfers between devices, local(): lax.all_to_all(back_rows, 'ep', split_axis=0, concat_axis=0, tiled=True)  10.4 us
    dot_general x1, matrix products, local(): lax.dot_general(columns, hidden, (((0,), (1,)), ((), ())), preferred_elem...  9.84 us
    dot_general x1, matrix products, local(): gate = jnp.dot(piece, gate_rows, preferred_element_type=jnp.float32)  6.54 us
    scatter-add x1, other arithmetic, local(): total.at[got_token.reshape(-1)]  6.41 us
  transfers between devices with their start and end apart: 4, of which 3 were waited for; matrix products, arithmetic and copies ran while one was open for 8% of the time, Pallas kernels for 0%

commit v1 on v0

--- a/solution.py
+++ b/solution.py
@@ -1,20 +1,294 @@
+import functools
+
 import jax
 import jax.numpy as jnp
 from jax import lax
+from jax.experimental import pallas as pl
+from jax.experimental.pallas import tpu as pltpu
 from jax.sharding import PartitionSpec as P
 
-D = 2048
+MESH = pl.DeviceIdType.MESH
+VMEM_BYTES = 67_043_328
+LANES = 128
+CHUNKS = 2
+
+
+def kernel(
+    ep, tp, chunks,
+    tok, gain, chosen, aff, wg_hbm, wu_hbm, wd_hbm,
+    out,
+    wg, wu, wd, full, normed, hidden, part, got1, got2, own, weighted,
+    near, back, got_back, chosen_row, aff_row, chosen_col, aff_col,
+    w_sem, z_send, z_recv, ag_send, ag_recv,
+    r1_send, r1_recv, r2_send, r2_recv, b_send, b_recv,
+):
+    me = lax.axis_index("ep")
+    t = lax.axis_index("tp")
+    tok_dev, width = tok.shape
+    rows, d = full.shape
+    count = chosen.shape[1]
+    size = rows // chunks
+    ff = wg.shape[1]
+    f32, bf16 = jnp.float32, jnp.bfloat16
+
+    def flip(m):
+        index, bit = t, 1
+        while bit <= m:
+            if m & bit:
+                index = index + bit - 2 * bit * ((t // bit) % 2)
+            bit *= 2
+        return index
+
+    def cols(m):
+        return pl.ds(pl.multiple_of(flip(m) * width, LANES), width)
+
+    def remote(src, dst, send, recv, ep_to, tp_to):
+        return pltpu.make_async_remote_copy(
+            src_ref=src, dst_ref=dst, send_sem=send, recv_sem=recv,
+            device_id=(ep_to, tp_to), device_id_type=MESH,
+        )
+
+    evens = list(range(2, tp, 2))
+    weights = [
+        pltpu.make_async_copy(h.at[0], v, w_sem.at[i])
+        for i, (h, v) in enumerate(((wg_hbm, wg), (wu_hbm, wu), (wd_hbm, wd)))
+    ]
+    for copy in weights:
+        copy.start()
+
+    barrier = pltpu.get_barrier_semaphore()
+    for m in [1] + evens:
+        pl.semaphore_signal(barrier, inc=1, device_id=(me, flip(m)), device_id_type=MESH)
+    for k in range(1, ep):
+        pl.semaphore_signal(
+            barrier, inc=1, device_id=(lax.rem(me + k, ep), t), device_id_type=MESH
+        )
+    pl.semaphore_wait(barrier, len(evens) + ep)
+
+    def z_copy(k):
+        return remote(
+            tok, near.at[k], z_send.at[k], z_recv.at[k], lax.rem(me + k, ep), t
+        )
+
+    for k in range(1, ep):
+        z_copy(k).start()
+
+    chosen_row[...] = jnp.full(chosen_row.shape, -1.0, f32)
+    aff_row[...] = jnp.zeros(aff_row.shape, f32)
+    chosen_row[:, :count] = chosen[...].astype(f32)
+    aff_row[:, :count] = aff[...]
+    diagonal = lax.broadcasted_iota(jnp.int32, (rows, rows), 0) == lax.broadcasted_iota(
+        jnp.int32, (rows, rows), 1
+    )
+    chosen_col[...] = jnp.sum(jnp.where(diagonal, chosen_row[...], 0.0), axis=1, keepdims=True)
+    aff_col[...] = jnp.sum(jnp.where(diagonal, aff_row[...], 0.0), axis=1, keepdims=True)
+
+    g = gain[...]
+    g0 = g.astype(bf16).astype(f32)
+    g1 = (g - g0).astype(bf16).astype(f32)
+    g2 = g - g0 - g1
+
+    order = list(range(chunks))[::-1]
+
+    def span(c):
+        return pl.ds(c * size, size)
+
+    def ag_copy(c, m, via):
+        block = full.at[span(c), cols(via)]
+        return remote(
+            block, block, ag_send.at[c, m], ag_recv.at[c, m], me, flip(m) if via == 0 else flip(1)
+        )
+
+    def ag_wait(c, m):
+        block = full.at[span(c), cols(m)]
+        remote(block, block, ag_send.at[c, m], ag_recv.at[c, m], me, flip(m)).wait_recv()
+
+    for k in range(1, ep):
+        z_copy(k).wait_recv()
+    lane_token = lax.broadcasted_iota(jnp.int32, (size, tok_dev), 1)
+    for c in order:
+        total = None
+        for k in range(ep):
+            source = lax.rem(me + ep - k, ep)
+            hot = (chosen_col[span(c), :] == (lane_token + source * tok_dev).astype(f32)).astype(f32)
+            block = tok[...] if k == 0 else near[k]
+            product = jnp.dot(hot.astype(bf16), block, preferred_element_type=f32)
+            total = product if total is None else total + product
+        if c == order[0]:
+            row = lax.broadcasted_iota(jnp.int32, (size, width), 0)
+            total = jnp.where(row == size - 3, g0, total)
+            total = jnp.where(row == size - 2, g1, total)
+            total = jnp.where(row == size - 1, g2, total)
+        full[span(c), cols(0)] = total.astype(bf16)
+        for m in evens + [1]:
+            ag_copy(c, m, 0).start()
+
+    def forward(c):
+        for m in evens:
+            ag_wait(c, m)
+            ag_copy(c, m + 1, m).start()
+
+    tile = min(ff, 256)
+    forward(order[0])
+    gain_all = None
+    for position, c in enumerate(order):
+        for m in range(1, tp, 2):
+            ag_wait(c, m)
+        if gain_all is None:
+            last = full[pl.ds(rows - 16, 16), :].astype(f32)
+            gain_all = (last[15:16, :] + last[14:15, :]) + last[13:14, :]
+        floats = full[span(c), :].astype(f32)
+        mean_square = jnp.sum(floats * floats, axis=1, keepdims=True) / d
+        normed[...] = (floats * lax.rsqrt(mean_square + EPS) * gain_all).astype(bf16)
+        if position == 0:
+            weights[0].wait()
+            weights[1].wait()
+
+        @pl.loop(0, ff // tile)
+        def _(j):
+            units = pl.ds(pl.multiple_of(j * tile, LANES), tile)
+            gate = jnp.dot(normed[...], wg[:, units], preferred_element_type=f32)
+            upward = jnp.dot(normed[...], wu[:, units], preferred_element_type=f32)
+            hidden[:, units] = (gate / (1.0 + jnp.exp(-gate)) * upward).astype(bf16)
+
+        if position + 1 < chunks:
+            forward(order[position + 1])
+        if position == 0:
+            weights[2].wait()
+
+        def down(m):
+            return jnp.dot(hidden[...], wd[:, cols(m)], preferred_element_type=f32)
+
+        for m in [e + 1 for e in evens] + [1]:
+            part[c, m] = down(m).astype(bf16)
+            remote(
+                part.at[c, m], got1.at[c, m - 1], r1_send.at[c, m], r1_recv.at[c, m - 1],
+                me, flip(1),
+            ).start()
+        for m in evens + [0]:
+            mine = down(m)
+            remote(
+                part.at[c, m + 1], got1.at[c, m], r1_send.at[c, m + 1], r1_recv.at[c, m],
+                me, flip(1),
+            ).wait_recv()
+            mine = mine + got1[c, m].astype(f32)
+            if m:
+                part[c, m] = mine.astype(bf16)
+                remote(
+                    part.at[c, m], got2.at[c, m], r2_send.at[c, m], r2_recv.at[c, m], me, flip(m)
+                ).start()
+            else:
+                own[span(c), :] = mine
+
+    for c in order:
+        total = own[span(c), :]
+        for m in evens:
+            remote(
+                part.at[c, m], got2.at[c, m], r2_send.at[c, m], r2_recv.at[c, m], me, flip(m)
+            ).wait_recv()
+            total = total + got2[c, m].astype(f32)
+        weighted[span(c), :] = (total * aff_col[span(c), :]).astype(bf16)
+
+    sub_token = lax.broadcasted_iota(jnp.int32, (tok_dev, rows), 0)
+
+    def at_tokens(owner):
+        hot = (chosen_row[...] == (sub_token + owner * tok_dev).astype(f32)).astype(f32)
+        return jnp.dot(hot.astype(bf16), weighted[...], preferred_element_type=f32)
+
+    def back_copy(k):
+        return remote(
+            back.at[k], got_back.at[k], b_send.at[k], b_recv.at[k], lax.rem(me + k, ep), t
+        )
+
+    for k in range(1, ep):
+        back[k] = at_tokens(lax.rem(me + k, ep)).astype(bf16)
+        back_copy(k).start()
+    mix = at_tokens(me)
+    for k in range(1, ep):
+        back_copy(k).wait_recv()
+        mix = mix + got_back[k].astype(f32)
+    out[...] = mix.astype(bf16)
+
+    for k in range(1, ep):
+        z_copy(k).wait_send()
+        back_copy(k).wait_send()
+    for c in order:
+        for m in evens + [1]:
+            ag_copy(c, m, 0).wait_send()
+        for m in evens:
+            ag_copy(c, m + 1, m).wait_send()
+            remote(
+                part.at[c, m], got2.at[c, m], r2_send.at[c, m], r2_recv.at[c, m], me, flip(m)
+            ).wait_send()
+        for m in range(1, tp, 2):
+            remote(
+                part.at[c, m], got1.at[c, m - 1], r1_send.at[c, m], r1_recv.at[c, m - 1],
+                me, flip(1),
+            ).wait_send()
+
+
+def fused(ep, tp, tokens, norm_gain, chosen, affinity, w_gate, w_up, w_down):
+    tok_dev, width = tokens.shape
+    d, ff = w_gate.shape[1:]
+    count = chosen.shape[1]
+    step = 16 * CHUNKS
+    rows = -(-(count + 3) // step) * step
+    size = rows // CHUNKS
+    f32, bf16 = jnp.float32, jnp.bfloat16
+    vmem = pl.BlockSpec(memory_space=pltpu.VMEM)
+    hbm = pl.BlockSpec(memory_space=pl.ANY)
+    dma = pltpu.SemaphoreType.DMA
+    return pl.pallas_call(
+        functools.partial(kernel, ep, tp, CHUNKS),
+        out_shape=jax.ShapeDtypeStruct((tok_dev, width), bf16),
+        in_specs=[vmem] * 4 + [hbm] * 3,
+        out_specs=vmem,
+        scratch_shapes=[
+            pltpu.VMEM((d, ff), bf16),
+            pltpu.VMEM((d, ff), bf16),
+            pltpu.VMEM((ff, d), bf16),
+            pltpu.VMEM((rows, d), bf16),
+            pltpu.VMEM((size, d), bf16),
+            pltpu.VMEM((size, ff), bf16),
+            pltpu.VMEM((CHUNKS, tp, size, width), bf16),
+            pltpu.VMEM((CHUNKS, tp, size, width), bf16),
+            pltpu.VMEM((CHUNKS, tp, size, width), bf16),
+            pltpu.VMEM((rows, width), f32),
+            pltpu.VMEM((rows, width), bf16),
+            pltpu.VMEM((ep, tok_dev, width), bf16),
+            pltpu.VMEM((ep, tok_dev, width), bf16),
+            pltpu.VMEM((ep, tok_dev, width), bf16),
+            pltpu.VMEM((1, rows), f32),
+            pltpu.VMEM((1, rows), f32),
+            pltpu.VMEM((rows, 1), f32),
+            pltpu.VMEM((rows, 1), f32),
+            dma((3,)),
+            dma((ep,)),
+            dma((ep,)),
+            dma((CHUNKS, tp)),
+            dma((CHUNKS, tp)),
+            dma((CHUNKS, tp)),
+            dma((CHUNKS, tp)),
+            dma((CHUNKS, tp)),
+            dma((CHUNKS, tp)),
+            dma((ep,)),
+            dma((ep,)),
+        ],
+        compiler_params=pltpu.CompilerParams(
+            collective_id=0, has_side_effects=True, vmem_limit_bytes=VMEM_BYTES
+        ),
+    )(tokens, norm_gain[None, :], chosen, affinity, w_gate, w_up, w_down)
 
 
 EPS = 1e-06
 
 
-def local(tokens, norm_gain, chosen, affinity, w_gate, w_up, w_down):
+def plain(tokens, norm_gain, chosen, affinity, w_gate, w_up, w_down):
     tok_dev, width_part = tokens.shape
     ep_count = lax.axis_size("ep")
     floats = tokens.astype(jnp.float32)
     square_sum = lax.psum(jnp.sum(floats * floats, axis=1), "tp")
-    normed = (floats * lax.rsqrt(square_sum / D + EPS)[:, None] * norm_gain[None, :]).astype(
+    normed = (floats * lax.rsqrt(square_sum / w_gate.shape[1] + EPS)[:, None] * norm_gain[None, :]).astype(
         jnp.bfloat16
     )
     own_choice = chosen[0]
@@ -62,6 +336,14 @@
 
 
 def solution(mesh):
+    ep, tp = mesh.shape["ep"], mesh.shape["tp"]
+
+    def local(tokens, *rest):
+        whole_lanes = tokens.shape[1] % LANES == 0 and rest[3].shape[2] % LANES == 0
+        if whole_lanes and tp >= 4 and tp & (tp - 1) == 0:
+            return fused(ep, tp, tokens, *rest)
+        return plain(tokens, *rest)
+
     in_specs = (
         P("ep", "tp"),
         P("tp"),

time: 160 us -> 58 us (0.36)
  waiting for transfers between devices: 64.4 us -> 0 us
  Pallas kernels: 0 us -> 56.3 us
  blocking collectives: 30.1 us -> 0 us
  matrix products: 16.4 us -> 0 us
  other arithmetic: 13.9 us -> 0 us
  between operations: 13.5 us -> 0.01 us
  local copies, waits for them, and re-layouts: 11.8 us -> 1.53 us
  starting transfers between devices: 9.24 us -> 0 us
    pallas_call x0 -> x1, Pallas kernels: none -> 56.3 us  [fused(): pl.pallas_call(functools.partial(kernel, ep, tp, CHUNKS), out_shape=jax.S...]
    reduce_scatter x1 -> x0, waiting for transfers between devices: 27.1 us -> none  [local(): lax.psum_scatter(lax.dot_general(columns, hidden, (((0,), (1,)), ((), ())...]
    all_gather x1 -> x0, waiting for transfers between devices: 26.9 us -> none  [local(): piece = lax.all_gather(picked, 'tp', axis=1, tiled=True)]
    dot_general x2 -> x0, matrix products: 16.4 us -> none  [the longest x1 9.84 us: local(): lax.dot_general(columns, hidden, (((0,), (1,)), ((), ())), preferred_elem...]
    psum x1 -> x0, blocking collectives: 15.2 us -> none  [local(): square_sum = lax.psum(jnp.sum(floats * floats, axis=1), 'tp')]
    all_gather x1 -> x0, blocking collectives: 15 us -> none  [local(): every_token = lax.all_gather(normed, 'ep', axis=0, tiled=True)]
    all_to_all x2 -> x0, waiting for transfers between devices: 10.4 us -> none  [the longest x1 10.4 us: local(): lax.all_to_all(back_rows, 'ep', split_axis=0, concat_axis=0, tiled=True)]
    gather x4 -> x0, local copies, waits for them, and re-layouts: 10.1 us -> none  [the longest x2 4.74 us: local(): back_token = jnp.where(back_filled, owner_local[back_pick], tok_dev)]
  transfers between devices with their start and end apart: 4 -> 0, of which waited for: 3 -> 0; matrix products, arithmetic and copies ran while one was open for 8% -> 0% of each run, Pallas kernels for 0% -> 0%
where the time goes in v1:
time: 58 us; the launch traced here: 57.8 us
  Pallas kernels  56.3 us (97%)
  local copies, waits for them, and re-layouts  1.53 us (3%)
    pallas_call x1, Pallas kernels, fused(): pl.pallas_call(functools.partial(kernel, ep, tp, CHUNKS), out_shape=jax.S...  56.3 us
    unnamed x1, local copies, waits for them, and re-layouts  1.53 us

profile of v1, /device:TPU:0, one launch (start us, length us, event | category | flops | bytes accessed | tf_op | source)
XLA Modules:
  0.0 57.8 jit_solution(16453971172312795705)
XLA Ops:
  0.0 56.3 %shard_map.73 = bf16[168,256]{1,0:T(8,128)(2,1)} custom-call(bf16[168,256]{1,0:T(8,128)(2,1)} %tok.1, f32[1,256]{1,0:T(1,128)} %bitcast.1, s32[1,504]{1,0:T(1,128)} %chosen.1, f32[1,504]{1,0:T(1,128)} %aff.1, bf16[1,2048,1024]{2,1,0:T(8,128)(2,1)} %wg_hbm.1, bf16[1,2048,1024]{2,1,0:T(8,128)(2,1)} %wu_hbm.1, bf16[1,1024,2048]{2,1,0:T(8,128)(2,1)} %wd_hbm.1), custom_call_target="tpu_custom_call" | custom-call | tf_op jit(solution)/shard_map/pallas_call | solution.py:241
  56.3 1.5 %copy.9 = bf16[168,256]{1,0:T(8,128)(2,1)} copy(bf16[168,256]{1,0:T(8,128)(2,1)} %shard_map.73) | data formatting | bytes 172032

commit v2 on v1

v2 whole, which is shorter than its diff:
```python
import functools

import jax
import jax.numpy as jnp
from jax import lax
from jax.experimental import pallas as pl
from jax.experimental.pallas import tpu as pltpu
from jax.sharding import PartitionSpec as P

MESH = pl.DeviceIdType.MESH
VMEM_BYTES = 67_043_328
LANES = 128
CHUNKS = 2
LAG = 1


def kernel(
    ep, tp, chunks,
    tok, gain, chosen, aff, wg_hbm, wu_hbm, wd_hbm,
    out,
    wg, wu, wd, full, normed, hidden, part, got1, got2, own, weighted,
    near, back, got_back, chosen_row, aff_row, aff_token, slot_row, slot_col,
    aff_col, gain_all, keep, w_sem, g_send, g_recv, z_send, z_recv, ag_send, ag_recv,
    r1_send, r1_recv, r2_send, r2_recv, b_send, b_recv,
):
    me = lax.axis_index("ep")
    t = lax.axis_index("tp")
    tok_dev, width = tok.shape
    rows = full.shape[1]
    d = wg.shape[0]
    count = chosen.shape[1]
    size = rows // chunks
    ff = wg.shape[1]
    f32, bf16 = jnp.float32, jnp.bfloat16

    def flip(m):
        index, bit = t, 1
        while bit <= m:
            if m & bit:
                index = index + bit - 2 * bit * ((t // bit) % 2)
            bit *= 2
        return index

    def cols(m):
        return pl.ds(pl.multiple_of(flip(m) * width, LANES), width)

    def remote(src, dst, send, recv, ep_to, tp_to):
        return pltpu.make_async_remote_copy(
            src_ref=src, dst_ref=dst, send_sem=send, recv_sem=recv,
            device_id=(ep_to, tp_to), device_id_type=MESH,
        )

    evens = [6, 2, 4]
    half = size // 2
    odds = [m + 1 for m in evens] + [1]
    order = list(range(chunks))
    weights = [
        pltpu.make_async_copy(h.at[0], v, w_sem.at[i])
        for i, (h, v) in enumerate(((wg_hbm, wg), (wu_hbm, wu), (wd_hbm, wd)))
    ]
    for copy in weights:
        copy.start()

    spare = ep * tok_dev - count
    need = [min(tok_dev, -(-(-(-(size * (c + 1) + spare) // ep)) // 16) * 16) for c in order]
    need[-1] = tok_dev
    least = [size * c // ep // 16 * 16 for c in order]
    done = [min(tok_dev, size * (c + 1) // ep // 16 * 16) for c in order]
    done[-1] = tok_dev

    def piece(ends, c):
        start = ends[c - 1] if c else 0
        return pl.ds(start, ends[c] - start)

    barrier = pltpu.get_barrier_semaphore()
    for m in range(1, tp):
        pl.semaphore_signal(barrier, inc=1, device_id=(me, flip(m)), device_id_type=MESH)
    for k in range(1, ep):
        pl.semaphore_signal(
            barrier, inc=1, device_id=(lax.rem(me + k, ep), t), device_id_type=MESH
        )
    pl.semaphore_wait(barrier, tp + ep - 2)

    def z_copy(c, k):
        rows_c = piece(need, c)
        return remote(
            tok.at[rows_c, :], near.at[k, rows_c, :], z_send.at[c, k], z_recv.at[c, k],
            lax.rem(me + k, ep), t,
        )

    for c in order:
        if piece(need, c).size:
            for k in range(1, ep):
                z_copy(c, k).start()

    def gain_copy(m):
        return remote(
            gain, gain_all.at[:, cols(0)], g_send.at[m], g_recv.at[m], me, flip(m)
        )

    def gain_wait(m):
        remote(gain, gain_all.at[:, cols(m)], g_send.at[m], g_recv.at[m], me, flip(m)).wait_recv()

    for m in range(1, tp):
        gain_copy(m).start()
    gain_all[:, cols(0)] = gain[...]

    chosen_row[...] = jnp.full(chosen_row.shape, -1.0, f32)
    aff_row[...] = jnp.zeros(aff_row.shape, f32)
    chosen_row[:, :count] = chosen[...].astype(f32)
    aff_row[:, :count] = aff[...]
    diagonal = lax.broadcasted_iota(jnp.int32, (rows, rows), 0) == lax.broadcasted_iota(
        jnp.int32, (rows, rows), 1
    )
    given = jnp.sum(jnp.where(diagonal, chosen_row[...], 0.0), axis=1, keepdims=True)
    factor = jnp.sum(jnp.where(diagonal, aff_row[...], 0.0), axis=1, keepdims=True)

    owners = [lax.rem(me + q, ep) for q in range(ep)]
    lane = lax.broadcasted_iota(jnp.int32, (rows, tok_dev), 1)
    sub = lax.broadcasted_iota(jnp.int32, (tok_dev, rows), 0)
    taken_row, taken_col = [], []
    for q in range(ep):
        match = given == (lane + owners[q] * tok_dev).astype(f32)
        taken_row.append(jnp.sum(match.astype(f32), axis=0, keepdims=True))
        aff_token[q] = jnp.sum(jnp.where(match, factor, 0.0), axis=0, keepdims=True)
        match = chosen_row[...] == (sub + owners[q] * tok_dev).astype(f32)
        taken_col.append(jnp.sum(match.astype(f32), axis=1, keepdims=True))
    down_index = lax.broadcasted_iota(jnp.int32, (tok_dev, tok_dev), 0) * ep
    across_index = lax.broadcasted_iota(jnp.int32, (tok_dev, tok_dev), 1) * ep
    for q in range(ep):
        ahead = jnp.zeros((tok_dev, tok_dev), f32)
        above = jnp.zeros((tok_dev, tok_dev), f32)
        for p in range(ep):
            ahead = ahead + jnp.where(
                down_index + owners[p] < across_index + owners[q], taken_col[p], 0.0
            )
            above = above + jnp.where(
                across_index + owners[p] < down_index + owners[q], taken_row[p], 0.0
            )
        slot_row[q] = jnp.where(taken_row[q] > 0, jnp.sum(ahead, axis=0, keepdims=True), -1.0)
        slot_col[q] = jnp.where(taken_col[q] > 0, jnp.sum(above, axis=1, keepdims=True), -1.0)

    def span(c):
        return pl.ds(c * size, size)

    routes = {
        1: (0, None, 1), 2: (0, None, 2), 4: (0, None, 4),
        3: (2, None, 1), 6: (2, 0, 4), 5: (4, None, 1), 8: (4, 1, 2),
        7: (6, 0, 1), 9: (6, 1, 1),
    }

    def ag_block(c, m, part_of):
        if part_of is None:
            return full.at[flip(m), span(c), :]
        return full.at[flip(m), pl.ds(c * size + part_of * half, half), :]

    def ag_copy(c, s):
        m, part_of, to = routes[s]
        block = ag_block(c, m, part_of)
        return remote(block, block, ag_send.at[c, s], ag_recv.at[c, s], me, flip(to))

    def ag_wait(c, s):
        m, part_of, to = routes[s]
        block = ag_block(c, m ^ to, part_of)
        remote(block, block, ag_send.at[c, s], ag_recv.at[c, s], me, flip(to)).wait_recv()

    def pick(c):
        if piece(need, c).size:
            for k in range(1, ep):
                z_copy(c, k).wait_recv()
        low, high = least[c], need[c]
        place = (lax.broadcasted_iota(jnp.int32, (size, high - low), 0) + c * size).astype(f32)
        total = jnp.zeros((size, width), f32)
        scale = jnp.zeros((size, high - low), f32)
        for k in range(ep):
            q = (ep - k) % ep
            hot = (place == slot_row[q, :, low:high]).astype(f32)
            scale = scale + hot * aff_token[q, :, low:high]
            block = tok[low:high, :] if k == 0 else near[k, low:high, :]
            total = total + jnp.dot(hot.astype(bf16), block, preferred_element_type=f32)
        aff_col[span(c), :] = jnp.sum(scale, axis=1, keepdims=True)
        full[t, span(c), :] = total.astype(bf16)
        for s in (2, 4, 1):
            ag_copy(c, s).start()

    def forward(c, stages):
        for s, onward in stages:
            ag_wait(c, s)
            for after in onward:
                ag_copy(c, after).start()

    first = ((2, (6, 3)), (4, (8, 5)))
    second = ((6, (7,)), (8, (9,)))

    sums = (
        (2, 0, 0, 2), (4, 1, 0, 4), (6, 0, 1, 2), (6, 1, 1, 4), (4, 0, 2, 4), (2, 1, 2, 2),
    )

    def r2_copy(c, s):
        m, part_of, slot, to = sums[s]
        rows_h = pl.ds(part_of * half, half)
        return remote(
            part.at[c, m, rows_h, :], got2.at[c, slot, rows_h, :],
            r2_send.at[c, s], r2_recv.at[c, s], me, flip(to),
        )

    def relay(c):
        for s, m, part_of in ((2, 4, 0), (3, 2, 1)):
            rows_h = pl.ds(part_of * half, half)
            r2_copy(c, s).wait_recv()
            part[c, m, rows_h, :] = (
                keep[c, part_of] + got2[c, 1, rows_h, :].astype(f32)
            ).astype(bf16)
            r2_copy(c, s + 2).start()

    def finish(c):
        for s in (0, 1, 4, 5):
            r2_copy(c, s).wait_recv()
        total = own[span(c), :] + got2[c, 0].astype(f32) + got2[c, 2].astype(f32)
        weighted[span(c), :] = (total * aff_col[span(c), :]).astype(bf16)
        if piece(done, c).size:
            for k in list(range(1, ep)) + [0]:
                at_tokens(c, k)

    def at_tokens(c, k):
        rows_c, slots = piece(done, c), size * (c + 1)
        place = lax.broadcasted_iota(jnp.int32, (rows_c.size, slots), 1).astype(f32)
        hot = (slot_col[k, rows_c, :] == place).astype(f32).astype(bf16)
        back[k, rows_c, :] = jnp.dot(
            hot, weighted[:slots, :], preferred_element_type=f32
        ).astype(bf16)
        if k:
            back_copy(c, k).start()

    def back_copy(c, k):
        rows_c = piece(done, c)
        return remote(
            back.at[k, rows_c, :], got_back.at[k, rows_c, :], b_send.at[c, k], b_recv.at[c, k],
            lax.rem(me + k, ep), t,
        )

    tile = min(ff, 256)
    pick(0)
    for c in order[1:]:
        pick(c)
        if c == 1:
            forward(0, first)
            forward(1, first)
            forward(0, second)
    for m in range(1, tp):
        gain_wait(m)
    for position, c in enumerate(order):
        for s in (1, 3, 5, 7, 9):
            ag_wait(c, s)
        square_sum = jnp.zeros((size, 1), f32)
        for b in range(tp):
            floats = full[b, span(c), :].astype(f32)
            square_sum = square_sum + jnp.sum(floats * floats, axis=1, keepdims=True)
        scale = lax.rsqrt(square_sum / d + EPS)
        for b in range(tp):
            at = slice(b * width, (b + 1) * width)
            floats = full[b, span(c), :].astype(f32)
            normed[:, at] = (floats * scale * gain_all[:, at]).astype(bf16)
        if position == 0:
            weights[0].wait()
            weights[1].wait()

        @pl.loop(0, ff // tile)
        def _(j):
            units = pl.ds(pl.multiple_of(j * tile, LANES), tile)
            gate = jnp.dot(normed[...], wg[:, units], preferred_element_type=f32)
            upward = jnp.dot(normed[...], wu[:, units], preferred_element_type=f32)
            hidden[:, units] = (gate / (1.0 + jnp.exp(-gate)) * upward).astype(bf16)

        if position + 1 < chunks:
            if position + 2 < chunks:
                forward(position + 2, first)
            forward(position + 1, second)
        if position:
            relay(position - 1)
        if position == 0:
            weights[2].wait()

        def down(m):
            return jnp.dot(hidden[...], wd[:, cols(m)], preferred_element_type=f32)

        for m in odds:
            part[c, m] = down(m).astype(bf16)
            remote(
                part.at[c, m], got1.at[c, m - 1], r1_send.at[c, m], r1_recv.at[c, m - 1],
                me, flip(1),
            ).start()
        for m in evens + [0]:
            mine = down(m)
            remote(
                part.at[c, m + 1], got1.at[c, m], r1_send.at[c, m + 1], r1_recv.at[c, m],
                me, flip(1),
            ).wait_recv()
            mine = mine + got1[c, m].astype(f32)
            if m == 6:
                part[c, 6] = mine.astype(bf16)
                r2_copy(c, 2).start()
                r2_copy(c, 3).start()
            elif m:
                part_of = 0 if m == 2 else 1
                sent, kept = pl.ds(part_of * half, half), (1 - part_of) * half
                part[c, m, sent, :] = mine[part_of * half : part_of * half + half].astype(bf16)
                r2_copy(c, part_of).start()
                keep[c, 1 - part_of] = mine[kept : kept + half]
            else:
                own[span(c), :] = mine

        if position >= LAG:
            finish(position - LAG)
    relay(chunks - 1)
    for c in order[max(0, chunks - LAG):]:
        finish(c)

    for c in order:
        if piece(done, c).size:
            rows_c = piece(done, c)
            mix = back[0, rows_c, :].astype(f32)
            for k in range(1, ep):
                back_copy(c, k).wait_recv()
                mix = mix + got_back[k, rows_c, :].astype(f32)
            out[rows_c, :] = mix.astype(bf16)

    for m in range(1, tp):
        gain_copy(m).wait_send()
    for c in order:
        for k in range(1, ep):
            if piece(need, c).size:
                z_copy(c, k).wait_send()
            if piece(done, c).size:
                back_copy(c, k).wait_send()
        for s in routes:
            ag_copy(c, s).wait_send()
        for s in range(len(sums)):
            r2_copy(c, s).wait_send()
        for m in odds:
            remote(
                part.at[c, m], got1.at[c, m - 1], r1_send.at[c, m], r1_recv.at[c, m - 1],
                me, flip(1),
            ).wait_send()


def fused(ep, tp, tokens, norm_gain, chosen, affinity, w_gate, w_up, w_down):
    tok_dev, width = tokens.shape
    d, ff = w_gate.shape[1:]
    count = chosen.shape[1]
    step = 32 * CHUNKS
    rows = -(-count // step) * step
    size = rows // CHUNKS
    f32, bf16 = jnp.float32, jnp.bfloat16
    vmem = pl.BlockSpec(memory_space=pltpu.VMEM)
    hbm = pl.BlockSpec(memory_space=pl.ANY)
    dma = pltpu.SemaphoreType.DMA
    return pl.pallas_call(
        functools.partial(kernel, ep, tp, CHUNKS),
        out_shape=jax.ShapeDtypeStruct((tok_dev, width), bf16),
        in_specs=[vmem] * 4 + [hbm] * 3,
        out_specs=vmem,
        scratch_shapes=[
            pltpu.VMEM((d, ff), bf16),
            pltpu.VMEM((d, ff), bf16),
            pltpu.VMEM((ff, d), bf16),
            pltpu.VMEM((tp, rows, width), bf16),
            pltpu.VMEM((size, d), bf16),
            pltpu.VMEM((size, ff), bf16),
            pltpu.VMEM((CHUNKS, tp, size, width), bf16),
            pltpu.VMEM((CHUNKS, tp, size, width), bf16),
            pltpu.VMEM((CHUNKS, tp, size, width), bf16),
            pltpu.VMEM((rows, width), f32),
            pltpu.VMEM((rows, width), bf16),
            pltpu.VMEM((ep, tok_dev, width), bf16),
            pltpu.VMEM((ep, tok_dev, width), bf16),
            pltpu.VMEM((ep, tok_dev, width), bf16),
            pltpu.VMEM((1, rows), f32),
            pltpu.VMEM((1, rows), f32),
            pltpu.VMEM((ep, 1, tok_dev), f32),
            pltpu.VMEM((ep, 1, tok_dev), f32),
            pltpu.VMEM((ep, tok_dev, 1), f32),
            pltpu.VMEM((rows, 1), f32),
            pltpu.VMEM((1, d), f32),
            pltpu.VMEM((CHUNKS, 2, size // 2, width), f32),
            dma((3,)),
            dma((tp,)),
            dma((tp,)),
            dma((CHUNKS, ep)),
            dma((CHUNKS, ep)),
            dma((CHUNKS, 2 * tp)),
            dma((CHUNKS, 2 * tp)),
            dma((CHUNKS, tp)),
            dma((CHUNKS, tp)),
            dma((CHUNKS, tp)),
            dma((CHUNKS, tp)),
            dma((CHUNKS, ep)),
            dma((CHUNKS, ep)),
        ],
        compiler_params=pltpu.CompilerParams(
            collective_id=0, has_side_effects=True, vmem_limit_bytes=VMEM_BYTES
        ),
    )(tokens, norm_gain[None, :], chosen, affinity, w_gate, w_up, w_down)


EPS = 1e-06


def plain(tokens, norm_gain, chosen, affinity, w_gate, w_up, w_down):
    tok_dev, width_part = tokens.shape
    ep_count = lax.axis_size("ep")
    floats = tokens.astype(jnp.float32)
    square_sum = lax.psum(jnp.sum(floats * floats, axis=1), "tp")
    normed = (floats * lax.rsqrt(square_sum / w_gate.shape[1] + EPS)[:, None] * norm_gain[None, :]).astype(
        jnp.bfloat16
    )
    own_choice = chosen[0]
    chosen_count = own_choice.shape[0]
    bound_rows = min(tok_dev, 2 * chosen_count // ep_count)
    slot_ids = jnp.arange(bound_rows, dtype=jnp.int32)
    positions = jnp.arange(chosen_count, dtype=jnp.int32)
    every_token = lax.all_gather(normed, "ep", axis=0, tiled=True)
    picked = every_token[own_choice]
    piece = lax.all_gather(picked, "tp", axis=1, tiled=True)
    gate_rows = w_gate[0]
    up_rows = w_up[0]
    gate = jnp.dot(piece, gate_rows, preferred_element_type=jnp.float32)
    upward = jnp.dot(piece, up_rows, preferred_element_type=jnp.float32)
    hidden = (jax.nn.silu(gate) * upward).astype(jnp.bfloat16)
    columns = w_down[0]
    summed = lax.psum_scatter(
        lax.dot_general(
            columns, hidden, (((0,), (1,)), ((), ())), preferred_element_type=jnp.float32
        ).astype(jnp.bfloat16),
        "tp",
        scatter_dimension=0,
        tiled=True,
    ).astype(jnp.float32)
    weighted = (summed * affinity[0][None, :]).astype(jnp.bfloat16).T
    owner = own_choice // tok_dev
    owner_local = own_choice - owner * tok_dev
    owner_hot = owner[:, None] == jnp.arange(ep_count, dtype=jnp.int32)[None, :]
    running = jnp.cumsum(owner_hot.astype(jnp.int32), axis=0)
    place = jnp.sum(jnp.where(owner_hot, running, 0), axis=1) - 1
    back_match = owner_hot.T[:, None, :] & (place[None, None, :] == slot_ids[None, :, None])
    back_filled = jnp.any(back_match, axis=2)
    back_pick = jnp.sum(jnp.where(back_match, positions[None, None, :], 0), axis=2)
    back_rows = jnp.where(back_filled[..., None], weighted[back_pick], jnp.zeros((), jnp.bfloat16))
    back_token = jnp.where(back_filled, owner_local[back_pick], tok_dev)
    got_back, got_token = (
        lax.all_to_all(back_rows, "ep", split_axis=0, concat_axis=0, tiled=True),
        lax.all_to_all(back_token, "ep", split_axis=0, concat_axis=0, tiled=True),
    )
    total = jnp.zeros((tok_dev, width_part), jnp.float32)
    total = total.at[got_token.reshape(-1)].add(
        got_back.reshape(-1, width_part).astype(jnp.float32), mode="drop"
    )
    return total.astype(jnp.bfloat16)


def solution(mesh):
    ep, tp = mesh.shape["ep"], mesh.shape["tp"]

    def local(tokens, *rest):
        whole_lanes = tokens.shape[1] % LANES == 0 and rest[3].shape[2] % LANES == 0
        if whole_lanes and tp == 2**3:
            return fused(ep, tp, tokens, *rest)
        return plain(tokens, *rest)

    in_specs = (
        P("ep", "tp"),
        P("tp"),
        P("ep", None),
        P("ep", None),
        P("ep", None, "tp"),
        P("ep", None, "tp"),
        P("ep", "tp", None),
    )
    out_specs = P("ep", "tp")
    return jax.shard_map(local, mesh=mesh, in_specs=in_specs, out_specs=out_specs, check_vma=False)
```

time: 58 us -> 53.9 us (0.929)
  Pallas kernels: 56.3 us -> 52.2 us
    pallas_call x1, Pallas kernels: 56.3 us -> 52.2 us  [fused(): pl.pallas_call(functools.partial(kernel, ep, tp, CHUNKS), out_shape=jax.S...]
where the time goes in v2:
time: 53.9 us; the launch traced here: 53.7 us
  Pallas kernels  52.2 us (97%)
  local copies, waits for them, and re-layouts  1.53 us (3%)
    pallas_call x1, Pallas kernels, fused(): pl.pallas_call(functools.partial(kernel, ep, tp, CHUNKS), out_shape=jax.S...  52.2 us
    unnamed x1, local copies, waits for them, and re-layouts  1.53 us

profile of v2, /device:TPU:0, one launch (start us, length us, event | category | flops | bytes accessed | tf_op | source)
XLA Modules:
  0.0 53.7 jit_solution(13035145761612852349)
XLA Ops:
  0.0 52.2 %shard_map.73 = bf16[168,256]{1,0:T(8,128)(2,1)} custom-call(bf16[168,256]{1,0:T(8,128)(2,1)} %tok.1, f32[1,256]{1,0:T(1,128)} %bitcast.1, s32[1,504]{1,0:T(1,128)} %chosen.1, f32[1,504]{1,0:T(1,128)} %aff.1, bf16[1,2048,1024]{2,1,0:T(8,128)(2,1)} %wg_hbm.1, bf16[1,2048,1024]{2,1,0:T(8,128)(2,1)} %wu_hbm.1, bf16[1,1024,2048]{2,1,0:T(8,128)(2,1)} %wd_hbm.1), custom_call_target="tpu_custom_call" | custom-call | tf_op jit(solution)/shard_map/pallas_call | solution.py:358
  52.2 1.5 %copy.9 = bf16[168,256]{1,0:T(8,128)(2,1)} copy(bf16[168,256]{1,0:T(8,128)(2,1)} %shard_map.73) | data formatting | bytes 172032
